TPU v7x, 256 devices: a whole 4x4x8 slice. The times are simulated.
256 devices in a mesh: fs: 32 (over z, x), tp: 8 (over y, core).
Axes of the slice: x: 4, y: 4, z: 8, core: 2. Of those that a mesh axis runs over, the one named last changes fastest.
Arguments:
- tokens: bfloat16 [32768, 2048], P(('fs', 'tp')), may hold values from -6 to 6
- gate_pre: bfloat16 [32768, 5632], P('fs', 'tp'), may hold values from -6 to 6
- value_pre: bfloat16 [32768, 5632], P('fs', 'tp'), may hold values from -6 to 6
- up_gate_w: bfloat16 [2048, 5632], P('fs', 'tp'), may hold values from -0.078125 to 0.078125
- up_value_w: bfloat16 [2048, 5632], P('fs', 'tp'), may hold values from -0.078125 to 0.078125
- conv_weight: float32 [3, 5632], P(None, 'tp'), may hold values from -3 to 3
- conv_bias: float32 [5632], P('tp'), may hold values from -3 to 3
- hidden_grad: bfloat16 [32768, 5632], P('fs', 'tp'), may hold values from -6 to 6
Outputs:
- input_grad: bfloat16 [32768, 2048], P(('fs', 'tp'))
- up_gate_grad: float32 [2048, 5632], P('fs', 'tp')
- up_value_grad: float32 [2048, 5632], P('fs', 'tp')
- conv_weight_grad: float32 [3, 5632], P(None, 'tp')
- conv_bias_grad: float32 [5632], P('tp')
All inputs are finite; a program needn't handle non-finite values.
Results may differ from a plain program's by a relative error of at most 0.013.
Values may be sent and summed in bfloat16 or wider, within the bound.
No kernel may reach another device: no remote copies, remote signals or barrier semaphores. Data moves between devices by JAX's collectives and lax.ppermute only.
A program may use at most 128 MiB of HBM per device.

v0:
```python
import jax
import jax.numpy as jnp
from jax import lax
from jax.sharding import Mesh
from jax.sharding import PartitionSpec as P

FS = ("fs_0", "fs_1")
FS_TP = ("fs_0", "fs_1", "tp")


def copy_for_each(shard, axis):
    peers = lax.axis_size(axis)
    return lax.all_to_all(
        jnp.broadcast_to(shard[None], (peers, *shard.shape)), axis, 0, 0, tiled=True
    )


def taken_together(shard, axis):
    return copy_for_each(shard, axis).sum(axis=0)


def in_one_piece(arrays, axis, dim, along):
    ends, at = ([], 0)
    for a in arrays[:-1]:
        at += a.shape[along]
        ends.append(at)
    both = jnp.concatenate(arrays, axis=along)
    return tuple(jnp.split(lax.all_gather(both, axis, axis=dim, tiled=True), ends, axis=along))


def summed_rows(subtotal, axes):
    return lax.psum_scatter(
        subtotal.astype(jnp.bfloat16), axes, scatter_dimension=0, tiled=True
    ).astype(jnp.float32)


def in_blocks(shard, dim, peers):
    lengths = shard.shape
    blocks = shard.reshape(*lengths[:dim], peers, lengths[dim] // peers, *lengths[dim + 1 :])
    return jnp.moveaxis(blocks, dim, 0)


def summed_on_arrival(shard, axis, dim):
    blocks = in_blocks(shard, dim, lax.axis_size(axis))
    arrived = lax.all_to_all(blocks, axis, split_axis=0, concat_axis=0, tiled=True)
    return arrived.astype(jnp.float32).sum(axis=0)


def contract_rows(left, right):
    return lax.dot_general(
        left, right, (((0,), (0,)), ((), ())), preferred_element_type=jnp.float32
    )


def contract_cols(left, right):
    return lax.dot_general(
        left, right, (((1,), (1,)), ((), ())), preferred_element_type=jnp.float32
    )


def on_device(
    tokens, gate_pre, value_pre, up_gate_w, up_value_w, conv_weight, conv_bias, hidden_grad
):
    length = gate_pre.shape[0]
    col_count = gate_pre.shape[1]
    scale = float(length * lax.axis_size(FS)) ** (-0.5)
    gate_float = gate_pre.astype(jnp.float32)
    padded = jnp.pad(gate_float, ((2, 0), (0, 0)))
    gate_conv = (
        conv_bias
        + conv_weight[0] * padded[:length]
        + conv_weight[1] * padded[1 : length + 1]
        + conv_weight[2] * padded[2:]
    )
    active, gelu_back = jax.vjp(jax.nn.gelu, gate_conv)
    grad_float = hidden_grad.astype(jnp.float32)
    value_grad = (grad_float * active).astype(jnp.bfloat16)
    conv_grad = gelu_back(grad_float * value_pre.astype(jnp.float32))[0]
    shifted = jnp.pad(conv_grad, ((0, 2), (0, 0)))
    gate_grad = (
        conv_weight[2] * conv_grad
        + conv_weight[1] * shifted[1 : length + 1]
        + conv_weight[0] * shifted[2:]
    ).astype(jnp.bfloat16)
    conv_terms = jnp.stack(
        [
            jnp.sum(conv_grad * padded[:length], axis=0),
            jnp.sum(conv_grad * padded[1 : length + 1], axis=0),
            jnp.sum(conv_grad * padded[2:], axis=0),
            jnp.sum(conv_grad, axis=0),
        ]
    )
    conv_total = taken_together(conv_terms, FS) * scale
    whole_tokens = lax.all_gather(tokens, "tp", axis=0, tiled=True)
    full_gate, full_value = in_one_piece((up_gate_w, up_value_w), FS, 0, 1)
    joined = summed_rows(
        jnp.concatenate(
            [contract_rows(whole_tokens, gate_grad), contract_rows(whole_tokens, value_grad)],
            axis=1,
        ),
        FS,
    )
    gate_out = joined[:, :col_count] * scale
    value_out = joined[:, col_count:] * scale
    input_grad = summed_on_arrival(
        (contract_cols(gate_grad, full_gate) + contract_cols(value_grad, full_value)).astype(
            jnp.bfloat16
        ),
        "tp",
        0,
    ).astype(jnp.bfloat16)
    return (input_grad, gate_out, value_out, conv_total[:3], conv_total[3])


def solution(mesh):
    finer = Mesh(mesh.devices.reshape(8, 4, mesh.shape["tp"]), ("fs_0", "fs_1", "tp"))
    in_specs = (
        P(FS_TP, None),
        P(FS, "tp"),
        P(FS, "tp"),
        P(FS, "tp"),
        P(FS, "tp"),
        P(None, "tp"),
        P("tp"),
        P(FS, "tp"),
    )
    out_specs = (P(FS_TP, None), P(FS, "tp"), P(FS, "tp"), P(None, "tp"), P("tp"))
    return jax.shard_map(
        on_device, mesh=finer, in_specs=in_specs, out_specs=out_specs, check_vma=False
    )
```

profile of v0, /device:TPU:8, one launch (start us, length us, event | category | flops | bytes accessed | tf_op | source)
XLA Modules:
  0.0 376.6 jit_solution(886776564580868433)
XLA Ops:
  7.2 0.0 copy-start
  7.2 0.0 copy-start.7
  7.2 0.0 copy-start.8
  7.2 0.0 copy-start.2
  7.2 0.0 all-gather.5.cloned.1.call-start
  7.3 0.7 all-gather.5.cloned.1.call-update
  7.9 0.0 all-gather.3.cloned.1.call-start
  8.0 1.8 pad_maximum_fusion.1
  9.8 0.0 all-gather.3.cloned.1.call-update
  9.8 0.0 reduce-scatter.4.cloned.1.call-start
  9.9 0.0 copy-start.3
  9.9 1.8 convert_element_type.30
  11.7 0.0 copy-done.7
  11.8 0.0 copy-done
  11.8 0.0 copy-done.8
  11.8 0.0 copy-done.2
  11.8 0.0 copy-done.3
  11.8 6.5 %multiply_reduce_fusion.2 = (f32[704]{0:T(1024)S(1)}, f32[704]{0:T(1024)S(1)}, f32[704]{0:T(1024)S(1)}, f32[704]{0:T(1024)S(1)}, f32[1024,704]{0,1:T(8,128)S(1)}, /*index=5*/f32[1024,704]{0,1:T(8,128)}) fusion(f32[1024,704]{0,1:T(8,128)S(1)} %convert_element_type.30, bf16[1024,704]{0,1:T(8,128)(2,1)S(1)} %copy-done, bf16[1024,704]{0,1:T(8,128)(2,1)S(1)} %copy-done.2, ...), kind=kLoop, calls=%fused_computation.31 | loop fusion | flops 25949440 | bytes 12998656 | tf_op jit(solution)/shard_map/reduce_sum | solution.py:87
  18.3 3.0 fusion.8
  21.3 25.0 %all-gather.5.cloned.1.call-done = bf16[1024,2048]{1,0:T(8,128)(2,1)} async-done(((bf16[128,2048]{1,0:T(8,128)(2,1)}), bf16[1024,2048]{1,0:T(8,128)(2,1)}) %all-gather.5.cloned.1.call-update) | async-done | bytes 4194320 | tf_op jit(solution)/shard_map/all_gather | solution.py:94
  46.4 5.9 %fusion.3 = bf16[2048,704]{0,1:T(8,128)(2,1)S(1)} fusion(bf16[1024,704]{0,1:T(8,128)(2,1)} %fusion.8, bf16[1024,2048]{1,0:T(8,128)(2,1)} %all-gather.5.cloned.1.call-done), kind=kOutput, calls=%fused_computation.15 | convolution fusion | flops 2954231808 | bytes 8519680 | tf_op jit(solution)/shard_map/dot_general | solution.py:50
  52.3 0.0 copy-done.1
  52.3 0.0 copy-done.4
  52.3 0.0 copy-done.10
  52.3 3.9 %fusion.4 = bf16[2048,704]{0,1:T(8,128)(2,1)S(1)} fusion(bf16[1024,2048]{1,0:T(8,128)(2,1)S(1)} %copy-done.10, bf16[1024,704]{0,1:T(8,128)(2,1)S(1)} %copy-done.4, f32[1024,704]{0,1:T(8,128)S(1)} %copy-done.1), kind=kOutput, calls=%fused_computation.16 | convolution fusion | flops 2962161664 | bytes 11403264 | tf_op jit(solution)/shard_map/dot_general | solution.py:50
  56.2 3.1 pad_maximum_fusion
  59.4 8.4 %copy.22 = bf16[2048,1408]{1,0:T(8,128)(2,1)} copy(bf16[2048,1408]{0,1:T(8,128)(2,1)} %pad_maximum_fusion) | data formatting | bytes 11534336
  67.8 0.0 reduce-scatter.4.cloned.1.call-update
  67.8 0.8 broadcast_in_dim.2
  68.6 10.0 %all-to-all-start.1 = ((f32[32,4,704]{2,1,0:T(4,128)}), f32[32,4,704]{2,1,0:T(4,128)S(1)}, u32[]{:S(2)}, u32[]{:S(2)}) async-start(f32[32,4,704]{2,1,0:T(4,128)} %broadcast_in_dim.2), calls=%async_computation.1 | async-start | bytes 786432 | tf_op jit(solution)/shard_map/all_to_all | solution.py:13
  78.7 60.2 %all-gather.3.cloned.1.call-done = bf16[2048,1408]{1,0:T(8,128)(2,1)} async-done(((bf16[64,1408]{1,0:T(8,128)(2,1)}), bf16[2048,1408]{1,0:T(8,128)(2,1)}) %all-gather.3.cloned.1.call-update) | async-done | bytes 5767184 | tf_op jit(solution)/shard_map/all_gather | solution.py:28
  138.9 6.0 %fusion.1 = f32[1024,2048]{1,0:T(8,128)S(1)} fusion(bf16[1024,704]{0,1:T(8,128)(2,1)} %fusion.8, bf16[2048,1408]{1,0:T(8,128)(2,1)} %all-gather.3.cloned.1.call-done), kind=kOutput, calls=%fused_computation.13 | convolution fusion | flops 2952790016 | bytes 12976128 | tf_op jit(solution)/shard_map/dot_general | solution.py:56
  144.9 0.0 copy-done.5
  144.9 0.0 copy-done.9
  144.9 7.6 %add_convert_fusion = bf16[1024,2048]{1,0:T(8,128)(2,1)} fusion(f32[1024,2048]{1,0:T(8,128)S(1)} %fusion.1, bf16[2048,1408]{1,0:T(8,128)(2,1)S(1)} %copy-done.9, bf16[1024,704]{0,1:T(8,128)(2,1)S(1)} %copy-done.5, f32[1024,704]{0,1:T(8,128)S(1)} %copy-done.1), kind=kOutput, calls=%fused_computation | convolution fusion | flops 2964914176 | bytes 20054016 | tf_op jit(solution)/shard_map/dot_general | solution.py:56
  152.5 0.0 all-to-all-done.1
  152.5 5.0 %all-to-all-start = ((bf16[8,128,2048]{2,1,0:T(8,128)(2,1)}), bf16[8,128,2048]{2,1,0:T(8,128)(2,1)}, u32[]{:S(2)}, u32[]{:S(2)}) async-start(bf16[8,128,2048]{2,1,0:T(8,128)(2,1)} %bitcast.11), calls=%async_computation | async-start | bytes 8388608 | tf_op jit(solution)/shard_map/all_to_all | solution.py:45
  157.4 0.1 reduce_sum.62
  157.5 0.0 copy-start.6
  157.5 0.6 slice_reduce_fusion
  158.1 47.6 %all-to-all-done = bf16[8,128,2048]{2,1,0:T(8,128)(2,1)} async-done(((bf16[8,128,2048]{2,1,0:T(8,128)(2,1)}), bf16[8,128,2048]{2,1,0:T(8,128)(2,1)}, u32[]{:S(2)}, u32[]{:S(2)}) %all-to-all-start) | async-done | bytes 4194336 | tf_op jit(solution)/shard_map/all_to_all | solution.py:45
  205.8 4.0 %reduce_sum.57 = bf16[128,2048]{1,0:T(8,128)(2,1)} reduce(bf16[8,128,2048]{2,1,0:T(8,128)(2,1)} %all-to-all-done, bf16[]{:T(256)} %constant.19.clone.1), dimensions={0}, to_apply=%region_0.1 | reduce | flops 1835008 | bytes 4718594 | tf_op jit(solution)/shard_map/reduce_sum | solution.py:46
  209.7 157.4 %reduce-scatter.4.cloned.1.call-done = bf16[64,1408]{1,0:T(8,128)(2,1)} async-done(((bf16[2048,1408]{1,0:T(8,128)(2,1)}), bf16[64,1408]{1,0:T(8,128)(2,1)}) %reduce-scatter.4.cloned.1.call-update) | async-done | bytes 180240
  367.2 1.1 copy.23
  368.4 0.0 copy-done.6
  368.4 0.1 slice_multiply_fusion
  368.4 0.8 copy.21
  369.3 0.8 copy.20
  (13 shorter events, 0.1 us)
Async XLA Ops:
  7.2 4.6 %copy-start = (bf16[1024,704]{0,1:T(8,128)(2,1)S(1)}, bf16[1024,704]{0,1:T(8,128)(2,1)}, u32[]{:S(2)}) copy-start(bf16[1024,704]{0,1:T(8,128)(2,1)} %param.9) | copy-start | bytes 4325380
  7.2 4.5 %copy-start.7 = (f32[3,704]{1,0:T(4,128)S(1)}, f32[3,704]{1,0:T(4,128)}, u32[]{:S(2)}) copy-start(f32[3,704]{1,0:T(4,128)} %param.13) | copy-start | bytes 25348
  7.2 4.6 %copy-start.8 = (f32[704]{0:T(1024)S(1)}, f32[704]{0:T(1024)}, u32[]{:S(2)}) copy-start(f32[704]{0:T(1024)} %param.14) | copy-start | bytes 8452
  7.2 4.6 %copy-start.2 = (bf16[1024,704]{0,1:T(8,128)(2,1)S(1)}, bf16[1024,704]{0,1:T(8,128)(2,1)}, u32[]{:S(2)}) copy-start(bf16[1024,704]{0,1:T(8,128)(2,1)} %param.10) | copy-start | bytes 4325380
  7.2 39.2 %all-gather.5.cloned.1.call-start = ((), (), s32[]{:S(2)}) async-start(), calls=%async_computation.4 | async-start | bytes 4718592 | tf_op jit(solution)/shard_map/all_gather | solution.py:94
  7.9 131.0 %all-gather.3.cloned.1.call-start = ((), (), s32[]{:S(2)}) async-start(), calls=%async_computation.3 | async-start | bytes 5947392 | tf_op jit(solution)/shard_map/all_gather | solution.py:28
  9.8 357.4 %reduce-scatter.4.cloned.1.call-start = ((), (), s32[]{:S(2)}) async-start(), calls=%async_computation.5 | async-start | bytes 5947392
  9.9 1.9 copy-start.3
  21.3 31.0 %copy-start.1 = (f32[1024,704]{0,1:T(8,128)S(1)}, f32[1024,704]{0,1:T(8,128)}, u32[]{:S(2)}) copy-start(f32[1024,704]{0,1:T(8,128)} %get-tuple-element.33) | copy-start | bytes 8650756
  46.4 5.9 %copy-start.4 = (bf16[1024,704]{0,1:T(8,128)(2,1)S(1)}, bf16[1024,704]{0,1:T(8,128)(2,1)}, u32[]{:S(2)}) copy-start(bf16[1024,704]{0,1:T(8,128)(2,1)} %param.15) | copy-start | bytes 4325380
  46.4 5.9 %copy-start.10 = (bf16[1024,2048]{1,0:T(8,128)(2,1)S(1)}, bf16[1024,2048]{1,0:T(8,128)(2,1)}, u32[]{:S(2)}) copy-start(bf16[1024,2048]{1,0:T(8,128)(2,1)} %all-gather.5.cloned.1.call-done) | copy-start | bytes 12582916
  68.6 83.8 %all-to-all-start.1 = ((f32[32,4,704]{2,1,0:T(4,128)}), f32[32,4,704]{2,1,0:T(4,128)S(1)}, u32[]{:S(2)}, u32[]{:S(2)}) async-start(f32[32,4,704]{2,1,0:T(4,128)} %broadcast_in_dim.2), calls=%async_computation.1 | async-start | bytes 786432 | tf_op jit(solution)/shard_map/all_to_all | solution.py:13
  138.9 6.0 %copy-start.5 = (bf16[1024,704]{0,1:T(8,128)(2,1)S(1)}, bf16[1024,704]{0,1:T(8,128)(2,1)}, u32[]{:S(2)}) copy-start(bf16[1024,704]{0,1:T(8,128)(2,1)} %param.15) | copy-start | bytes 4325380
  138.9 6.0 %copy-start.9 = (bf16[2048,1408]{1,0:T(8,128)(2,1)S(1)}, bf16[2048,1408]{1,0:T(8,128)(2,1)}, u32[]{:S(2)}) copy-start(bf16[2048,1408]{1,0:T(8,128)(2,1)} %all-gather.3.cloned.1.call-done) | copy-start | bytes 17301508
  152.5 53.3 %all-to-all-start = ((bf16[8,128,2048]{2,1,0:T(8,128)(2,1)}), bf16[8,128,2048]{2,1,0:T(8,128)(2,1)}, u32[]{:S(2)}, u32[]{:S(2)}) async-start(bf16[8,128,2048]{2,1,0:T(8,128)(2,1)} %bitcast.11), calls=%async_computation | async-start | bytes 8388608 | tf_op jit(solution)/shard_map/all_to_all | solution.py:45
  157.5 210.8 %copy-start.6 = (f32[4,704]{1,0:T(4,128)}, f32[4,704]{1,0:T(4,128)S(1)}, u32[]{:S(2)}) copy-start(f32[4,704]{1,0:T(4,128)S(1)} %broadcast_multiply_fusion) | copy-start | bytes 33796
Sparse Core Ops, SparseCore 0:
  9.9 36.4 all-gather.4
  49.5 89.3 all-gather.2
  142.9 224.2 reduce-scatter.3
where the time goes:
time: 377 us
  waiting for transfers between devices  291 us (77%)
  matrix products  23.3 us (6%)
  other arithmetic  20.5 us (5%)
  starting transfers between devices  15.1 us (4%)
  between operations  14 us (4%)
  local copies, waits for them, and re-layouts  12.7 us (3%)
    unnamed x4, waiting for transfers between devices  158 us
    all_gather x1, waiting for transfers between devices, in_one_piece(): lax.all_gather(both, axis, axis=dim, tiled=True)  60.2 us
    all_to_all x1, waiting for transfers between devices, summed_on_arrival(): lax.all_to_all(blocks, axis, split_axis=0, concat_axis=0, tiled=True)  47.6 us
    all_gather x1, waiting for transfers between devices, on_device(): whole_tokens = lax.all_gather(tokens, 'tp', axis=0, tiled=True)  25 us
    dot_general x2, matrix products, contract_cols(): lax.dot_general(left, right, (((1,), (1,)), ((), ())), preferred_element_...  13.5 us
    unnamed x26, local copies, waits for them, and re-layouts  11.2 us
    all_to_all x1, starting transfers between devices, copy_for_each(): lax.all_to_all(jnp.broadcast_to(shard[None], (peers, *shard.shape)), axis...  10 us
    dot_general x2, matrix products, contract_rows(): lax.dot_general(left, right, (((0,), (0,)), ((), ())), preferred_element_...  9.78 us
  transfers between devices with their start and end apart: 5, of which 4 were waited for; matrix products, arithmetic and copies ran while one was open for 14% of the time, Pallas kernels for 0%

commit v1 on v0

--- a/solution.py
+++ b/solution.py
@@ -6,6 +6,24 @@
 
 FS = ("fs_0", "fs_1")
 FS_TP = ("fs_0", "fs_1", "tp")
+
+
+def collect(array, axis, dim):
+    ways, here, lap = (lax.axis_size(axis), lax.axis_index(axis), array.shape[dim])
+    lengths = [n * ways if d == dim else n for d, n in enumerate(array.shape)]
+    full = lax.dynamic_update_slice_in_dim(
+        jnp.zeros(lengths, array.dtype), array, here * lap, axis=dim
+    )
+    going_up = going_down = array
+    for far in range(1, ways // 2 + 1):
+        going_up = lax.ppermute(going_up, axis, [(d, (d + 1) % ways) for d in range(ways)])
+        full = lax.dynamic_update_slice_in_dim(full, going_up, (here - far) % ways * lap, axis=dim)
+        if 2 * far < ways:
+            going_down = lax.ppermute(going_down, axis, [(d, (d - 1) % ways) for d in range(ways)])
+            full = lax.dynamic_update_slice_in_dim(
+                full, going_down, (here + far) % ways * lap, axis=dim
+            )
+    return full
 
 
 def copy_for_each(shard, axis):
@@ -91,7 +109,7 @@
         ]
     )
     conv_total = taken_together(conv_terms, FS) * scale
-    whole_tokens = lax.all_gather(tokens, "tp", axis=0, tiled=True)
+    whole_tokens = collect(tokens, "tp", 0)
     full_gate, full_value = in_one_piece((up_gate_w, up_value_w), FS, 0, 1)
     joined = summed_rows(
         jnp.concatenate(

time: 377 us -> 352 us (0.934)
  waiting for transfers between devices: 291 us -> 245 us
  local copies, waits for them, and re-layouts: 12.7 us -> 24 us
  starting transfers between devices: 15.1 us -> 21.9 us
    unnamed x4 -> x3, waiting for transfers between devices: 158 us -> 210 us
    all_to_all x1, waiting for transfers between devices: 47.6 us -> 0.01 us  [summed_on_arrival(): lax.all_to_all(blocks, axis, split_axis=0, concat_axis=0, tiled=True)]
    all_gather x1, waiting for transfers between devices: 60.2 us -> 26.6 us  [in_one_piece(): lax.all_gather(both, axis, axis=dim, tiled=True)]
    all_gather x1 -> x0, waiting for transfers between devices: 25 us -> none  [on_device(): whole_tokens = lax.all_gather(tokens, 'tp', axis=0, tiled=True)]
    ppermute x0 -> x7, waiting for transfers between devices: none -> 9.28 us  [the longest x4 8.56 us: collect(): lax.ppermute(going_up, axis, [(d, (d + 1) % ways) for d in range(ways)])]
    dynamic_update_slice x0 -> x8, local copies, waits for them, and re-layouts: none -> 8.95 us  [the longest x4 5.54 us: collect(): lax.dynamic_update_slice_in_dim(full, going_up, (here - far) % ways * lap...]
    ppermute x0 -> x7, starting transfers between devices: none -> 5.27 us  [the longest x3 5.24 us: collect(): lax.ppermute(going_down, axis, [(d, (d - 1) % ways) for d in range(ways)])]
    unnamed x26 -> x28, local copies, waits for them, and re-layouts: 11.2 us -> 11.1 us
  transfers between devices with their start and end apart: 5 -> 11, of which waited for: 4 -> 6; matrix products, arithmetic and copies ran while one was open for 14% -> 18% of each run, Pallas kernels for 0% -> 0%
where the time goes in v1:
time: 352 us; the launch traced here: 351 us
  waiting for transfers between devices  245 us (70%)
  matrix products  25.3 us (7%)
  local copies, waits for them, and re-layouts  24 us (7%)
  starting transfers between devices  21.9 us (6%)
  other arithmetic  20.2 us (6%)
  between operations  14.3 us (4%)
    unnamed x3, waiting for transfers between devices  210 us
    all_gather x1, waiting for transfers between devices, in_one_piece(): lax.all_gather(both, axis, axis=dim, tiled=True)  26.6 us
    dot_general x2, matrix products, contract_cols(): lax.dot_general(left, right, (((1,), (1,)), ((), ())), preferred_element_...  13.5 us
    dot_general x2, matrix products, contract_rows(): lax.dot_general(left, right, (((0,), (0,)), ((), ())), preferred_element_...  11.7 us
    all_to_all x1, starting transfers between devices, copy_for_each(): lax.all_to_all(jnp.broadcast_to(shard[None], (peers, *shard.shape)), axis...  11.6 us
    unnamed x28, local copies, waits for them, and re-layouts  11.1 us
    ppermute x4, waiting for transfers between devices, collect(): lax.ppermute(going_up, axis, [(d, (d + 1) % ways) for d in range(ways)])  8.56 us
  transfers between devices with their start and end apart: 11, of which 6 were waited for; matrix products, arithmetic and copies ran while one was open for 18% of the time, Pallas kernels for 0%

profile of v1, /device:TPU:8, one launch (start us, length us, event | category | flops | bytes accessed | tf_op | source)
XLA Modules:
  0.0 351.1 jit_solution(15994006144743202194)
XLA Ops:
  7.2 0.0 all-gather.2.cloned.1.call-start
  7.2 1.7 pad_maximum_fusion.1
  8.9 0.0 all-gather.2.cloned.1.call-update
  9.0 0.0 reduce-scatter.4.cloned.1.call-start
  9.0 0.0 copy-start
  9.0 0.0 copy-start.2
  9.0 0.0 copy-start.3
  9.1 0.0 collective-permute-start
  9.1 1.7 collective-permute-start.1
  10.8 1.7 convert_element_type.30
  12.6 6.5 %multiply_reduce_fusion.2 = (f32[704]{0:T(1024)S(1)}, f32[704]{0:T(1024)S(1)}, f32[704]{0:T(1024)S(1)}, f32[704]{0:T(1024)S(1)}, f32[1024,704]{0,1:T(8,128)S(1)}, /*index=5*/f32[1024,704]{0,1:T(8,128)}) fusion(f32[1024,704]{0,1:T(8,128)S(1)} %convert_element_type.30, bf16[1024,704]{0,1:T(8,128)(2,1)S(1)} %copy-done, bf16[1024,704]{0,1:T(8,128)(2,1)S(1)} %copy-done.2, ...), kind=kLoop, calls=%fused_computation.29 | loop fusion | flops 25949440 | bytes 12998656 | tf_op jit(solution)/shard_map/reduce_sum | solution.py:105
  19.2 3.0 fusion.6
  22.1 1.7 collective-permute-start.3
  23.9 2.5 broadcast_in_dim.4
  26.4 0.9 constant_dynamic-update-slice_fusion.7
  27.3 0.8 collective-permute-done.2
  28.1 0.0 collective-permute-start.4
  28.1 1.9 constant_dynamic-update-slice_fusion.6
  30.0 0.8 constant_dynamic-update-slice_fusion.5
  30.8 0.0 collective-permute-done.3
  30.8 1.8 collective-permute-start.5
  32.6 1.9 constant_dynamic-update-slice_fusion.4
  34.5 2.4 collective-permute-done.4
  36.9 0.8 constant_dynamic-update-slice_fusion.3
  37.8 0.8 constant_dynamic-update-slice_fusion.2
  38.6 0.7 collective-permute-done.5
  39.3 0.9 constant_dynamic-update-slice_fusion.1
  40.2 5.3 %collective-permute-done.6 = bf16[128,2048]{1,0:T(8,128)(2,1)S(1)} collective-permute-done((bf16[128,2048]{1,0:T(8,128)(2,1)S(1)}, bf16[128,2048]{1,0:T(8,128)(2,1)S(1)}, u32[]{:S(2)}, u32[]{:S(2)}) %collective-permute-start.6) | collective-permute-done | bytes 524320 | tf_op jit(solution)/shard_map/ppermute | solution.py:19
  45.5 0.9 constant_dynamic-update-slice_fusion
  46.4 5.7 %convolution_convert_fusion.1 = bf16[2048,704]{0,1:T(8,128)(2,1)S(1)} fusion(bf16[1024,704]{0,1:T(8,128)(2,1)S(1)} %copy-done.6, bf16[1024,2048]{1,0:T(8,128)(2,1)} %constant_dynamic-update-slice_fusion), kind=kOutput, calls=%fused_computation.7 | convolution fusion | flops 2954231808 | bytes 8519680 | tf_op jit(solution)/shard_map/dot_general | solution.py:68
  52.2 6.0 %convolution_convert_fusion = bf16[2048,704]{0,1:T(8,128)(2,1)S(1)} fusion(bf16[1024,2048]{1,0:T(8,128)(2,1)} %constant_dynamic-update-slice_fusion, bf16[1024,704]{0,1:T(8,128)(2,1)S(1)} %copy-done.4, f32[1024,704]{0,1:T(8,128)S(1)} %copy-done.1), kind=kOutput, calls=%fused_computation.6 | convolution fusion | flops 2962161664 | bytes 11403264 | tf_op jit(solution)/shard_map/dot_general | solution.py:68
  58.2 3.1 pad_maximum_fusion
  61.4 8.3 %copy.22 = bf16[2048,1408]{1,0:T(8,128)(2,1)} copy(bf16[2048,1408]{0,1:T(8,128)(2,1)} %pad_maximum_fusion) | data formatting | bytes 11534336
  69.6 0.0 reduce-scatter.4.cloned.1.call-update
  69.7 0.8 broadcast_in_dim.5
  70.5 11.6 %all-to-all-start.1 = ((f32[32,4,704]{2,1,0:T(4,128)}), f32[32,4,704]{2,1,0:T(4,128)S(1)}, u32[]{:S(2)}, u32[]{:S(2)}) async-start(f32[32,4,704]{2,1,0:T(4,128)} %broadcast_in_dim.5), calls=%async_computation.1 | async-start | bytes 786432 | tf_op jit(solution)/shard_map/all_to_all | solution.py:31
  82.2 26.6 %all-gather.2.cloned.1.call-done = bf16[2048,1408]{1,0:T(8,128)(2,1)} async-done(((bf16[64,1408]{1,0:T(8,128)(2,1)}), bf16[2048,1408]{1,0:T(8,128)(2,1)}) %all-gather.2.cloned.1.call-update) | async-done | bytes 5767184 | tf_op jit(solution)/shard_map/all_gather | solution.py:46
  108.7 6.0 %fusion.1 = f32[1024,2048]{1,0:T(8,128)S(1)} fusion(bf16[1024,704]{0,1:T(8,128)(2,1)} %fusion.6, bf16[2048,1408]{1,0:T(8,128)(2,1)} %all-gather.2.cloned.1.call-done), kind=kOutput, calls=%fused_computation.13 | convolution fusion | flops 2952790016 | bytes 12976128 | tf_op jit(solution)/shard_map/dot_general | solution.py:74
  114.7 7.6 %add_convert_fusion = bf16[1024,2048]{1,0:T(8,128)(2,1)} fusion(f32[1024,2048]{1,0:T(8,128)S(1)} %fusion.1, bf16[2048,1408]{1,0:T(8,128)(2,1)S(1)} %copy-done.11, bf16[1024,704]{0,1:T(8,128)(2,1)S(1)} %copy-done.5, f32[1024,704]{0,1:T(8,128)S(1)} %copy-done.1), kind=kOutput, calls=%fused_computation | convolution fusion | flops 2964914176 | bytes 20054016 | tf_op jit(solution)/shard_map/dot_general | solution.py:74
  122.3 4.9 %all-to-all-start = ((bf16[8,128,2048]{2,1,0:T(8,128)(2,1)}), bf16[8,128,2048]{2,1,0:T(8,128)(2,1)}, u32[]{:S(2)}, u32[]{:S(2)}) async-start(bf16[8,128,2048]{2,1,0:T(8,128)(2,1)} %bitcast.7), calls=%async_computation | async-start | bytes 8388608 | tf_op jit(solution)/shard_map/all_to_all | solution.py:63
  127.2 0.1 reduce_sum.62
  127.3 0.6 slice_reduce_fusion
  127.9 209.5 %reduce-scatter.4.cloned.1.call-done = bf16[64,1408]{1,0:T(8,128)(2,1)} async-done(((bf16[2048,1408]{1,0:T(8,128)(2,1)}), bf16[64,1408]{1,0:T(8,128)(2,1)}) %reduce-scatter.4.cloned.1.call-update) | async-done | bytes 180240
  337.4 1.1 copy.23
  338.6 0.1 slice_multiply_fusion
  338.7 0.8 copy.20
  339.5 0.8 copy.21
  340.4 3.8 %reduce_sum.57 = bf16[128,2048]{1,0:T(8,128)(2,1)} reduce(bf16[8,128,2048]{2,1,0:T(8,128)(2,1)} %all-to-all-done, bf16[]{:T(256)} %constant.67.clone.1), dimensions={0}, to_apply=%region_0.1 | reduce | flops 1835008 | bytes 4718594 | tf_op jit(solution)/shard_map/reduce_sum | solution.py:64
  (35 shorter events, 0.2 us)
Async XLA Ops:
  7.2 5.4 %copy-start.9 = (f32[3,704]{1,0:T(4,128)S(1)}, f32[3,704]{1,0:T(4,128)}, u32[]{:S(2)}) copy-start(f32[3,704]{1,0:T(4,128)} %param.13) | copy-start | bytes 25348
  7.2 5.4 %copy-start.10 = (f32[704]{0:T(1024)S(1)}, f32[704]{0:T(1024)}, u32[]{:S(2)}) copy-start(f32[704]{0:T(1024)} %param.14) | copy-start | bytes 8452
  7.2 101.5 %all-gather.2.cloned.1.call-start = ((), (), s32[]{:S(2)}) async-start(), calls=%async_computation.3 | async-start | bytes 5947392 | tf_op jit(solution)/shard_map/all_gather | solution.py:46
  9.0 328.5 %reduce-scatter.4.cloned.1.call-start = ((), (), s32[]{:S(2)}) async-start(), calls=%async_computation.4 | async-start | bytes 5947392
  9.0 3.6 %copy-start = (bf16[1024,704]{0,1:T(8,128)(2,1)S(1)}, bf16[1024,704]{0,1:T(8,128)(2,1)}, u32[]{:S(2)}) copy-start(bf16[1024,704]{0,1:T(8,128)(2,1)} %param.9) | copy-start | bytes 4325380
  9.0 3.6 %copy-start.2 = (bf16[1024,704]{0,1:T(8,128)(2,1)S(1)}, bf16[1024,704]{0,1:T(8,128)(2,1)}, u32[]{:S(2)}) copy-start(bf16[1024,704]{0,1:T(8,128)(2,1)} %param.10) | copy-start | bytes 4325380
  9.0 3.6 %copy-start.3 = (bf16[1024,704]{0,1:T(8,128)(2,1)S(1)}, bf16[1024,704]{0,1:T(8,128)(2,1)}, u32[]{:S(2)}) copy-start(bf16[1024,704]{0,1:T(8,128)(2,1)} %param.15) | copy-start | bytes 4325380
  9.1 10.1 %collective-permute-start = (bf16[128,2048]{1,0:T(8,128)(2,1)}, bf16[128,2048]{1,0:T(8,128)(2,1)}, u32[]{:S(2)}, u32[]{:S(2)}) collective-permute-start(bf16[128,2048]{1,0:T(8,128)(2,1)} %param.8), channel_id=1, source_target_pairs={{0,1},{1,2},{2,3},{3,4},{4,5},{5,6},{6,7},{7,0},{8,9},{9,10},{10,1... | collective-permute-start | bytes 1572872 | tf_op jit(solution)/shard_map/ppermute | solution.py:19
  9.1 13.1 %collective-permute-start.1 = (bf16[128,2048]{1,0:T(8,128)(2,1)}, bf16[128,2048]{1,0:T(8,128)(2,1)S(1)}, u32[]{:S(2)}, u32[]{:S(2)}) collective-permute-start(bf16[128,2048]{1,0:T(8,128)(2,1)} %param.8), channel_id=1, source_target_pairs={{0,7},{1,0},{2,1},{3,2},{4,3},{5,4},{6,5},{7,6},{8,15},{9,8},{10,9... | collective-permute-start | bytes 1572872 | tf_op jit(solution)/shard_map/ppermute | solution.py:22
  19.2 8.9 %collective-permute-start.2 = (bf16[128,2048]{1,0:T(8,128)(2,1)}, bf16[128,2048]{1,0:T(8,128)(2,1)}, u32[]{:S(2)}, u32[]{:S(2)}) collective-permute-start(bf16[128,2048]{1,0:T(8,128)(2,1)} %collective-permute-done), channel_id=1, source_target_pairs={{0,1},{1,2},{2,3},{3,4},{4,5},{5,6},{6,7},{7,0},{8,9},{9,10},{10,1... | collective-permute-start | bytes 1572872 | tf_op jit(solution)/shard_map/ppermute | solution.py:19
  22.1 4.3 %copy-start.7 = (bf16[128,2048]{1,0:T(8,128)(2,1)S(1)}, bf16[128,2048]{1,0:T(8,128)(2,1)}, u32[]{:S(2)}) copy-start(bf16[128,2048]{1,0:T(8,128)(2,1)} %param.8) | copy-start | bytes 1572868
  22.1 8.7 %collective-permute-start.3 = (bf16[128,2048]{1,0:T(8,128)(2,1)S(1)}, bf16[128,2048]{1,0:T(8,128)(2,1)S(1)}, u32[]{:S(2)}, u32[]{:S(2)}) collective-permute-start(bf16[128,2048]{1,0:T(8,128)(2,1)S(1)} %collective-permute-done.1), channel_id=1, source_target_pairs={{0,7},{1,0},{2,1},{3,2},{4,3},{5,4},{6,5},{7,6},{8,15},{9,8},{10,9... | collective-permute-start | bytes 1572872 | tf_op jit(solution)/shard_map/ppermute | solution.py:22
  28.1 8.8 %collective-permute-start.4 = (bf16[128,2048]{1,0:T(8,128)(2,1)}, bf16[128,2048]{1,0:T(8,128)(2,1)S(1)}, u32[]{:S(2)}, u32[]{:S(2)}) collective-permute-start(bf16[128,2048]{1,0:T(8,128)(2,1)} %collective-permute-done.2), channel_id=1, source_target_pairs={{0,1},{1,2},{2,3},{3,4},{4,5},{5,6},{6,7},{7,0},{8,9},{9,10},{10,1... | collective-permute-start | bytes 1572872 | tf_op jit(solution)/shard_map/ppermute | solution.py:19
  30.8 15.6 %copy-start.6 = (bf16[1024,704]{0,1:T(8,128)(2,1)S(1)}, bf16[1024,704]{0,1:T(8,128)(2,1)}, u32[]{:S(2)}) copy-start(bf16[1024,704]{0,1:T(8,128)(2,1)} %fusion.6) | copy-start | bytes 4325380
  30.8 8.5 %collective-permute-start.5 = (bf16[128,2048]{1,0:T(8,128)(2,1)S(1)}, bf16[128,2048]{1,0:T(8,128)(2,1)S(1)}, u32[]{:S(2)}, u32[]{:S(2)}) collective-permute-start(bf16[128,2048]{1,0:T(8,128)(2,1)S(1)} %collective-permute-done.3), channel_id=1, source_target_pairs={{0,7},{1,0},{2,1},{3,2},{4,3},{5,4},{6,5},{7,6},{8,15},{9,8},{10,9... | collective-permute-start | bytes 1572872 | tf_op jit(solution)/shard_map/ppermute | solution.py:22
  36.9 8.6 %collective-permute-start.6 = (bf16[128,2048]{1,0:T(8,128)(2,1)S(1)}, bf16[128,2048]{1,0:T(8,128)(2,1)S(1)}, u32[]{:S(2)}, u32[]{:S(2)}) collective-permute-start(bf16[128,2048]{1,0:T(8,128)(2,1)S(1)} %collective-permute-done.4), channel_id=1, source_target_pairs={{0,1},{1,2},{2,3},{3,4},{4,5},{5,6},{6,7},{7,0},{8,9},{9,10},{10,1... | collective-permute-start | bytes 1572872 | tf_op jit(solution)/shard_map/ppermute | solution.py:19
  46.4 5.8 %copy-start.1 = (f32[1024,704]{0,1:T(8,128)S(1)}, f32[1024,704]{0,1:T(8,128)}, u32[]{:S(2)}) copy-start(f32[1024,704]{0,1:T(8,128)} %get-tuple-element.33) | copy-start | bytes 8650756
  46.4 5.8 %copy-start.4 = (bf16[1024,704]{0,1:T(8,128)(2,1)S(1)}, bf16[1024,704]{0,1:T(8,128)(2,1)}, u32[]{:S(2)}) copy-start(bf16[1024,704]{0,1:T(8,128)(2,1)} %param.15) | copy-start | bytes 4325380
  70.5 51.8 %all-to-all-start.1 = ((f32[32,4,704]{2,1,0:T(4,128)}), f32[32,4,704]{2,1,0:T(4,128)S(1)}, u32[]{:S(2)}, u32[]{:S(2)}) async-start(f32[32,4,704]{2,1,0:T(4,128)} %broadcast_in_dim.5), calls=%async_computation.1 | async-start | bytes 786432 | tf_op jit(solution)/shard_map/all_to_all | solution.py:31
  108.7 6.0 %copy-start.5 = (bf16[1024,704]{0,1:T(8,128)(2,1)S(1)}, bf16[1024,704]{0,1:T(8,128)(2,1)}, u32[]{:S(2)}) copy-start(bf16[1024,704]{0,1:T(8,128)(2,1)} %param.15) | copy-start | bytes 4325380
  108.7 6.0 %copy-start.11 = (bf16[2048,1408]{1,0:T(8,128)(2,1)S(1)}, bf16[2048,1408]{1,0:T(8,128)(2,1)}, u32[]{:S(2)}) copy-start(bf16[2048,1408]{1,0:T(8,128)(2,1)} %all-gather.2.cloned.1.call-done) | copy-start | bytes 17301508
  122.3 218.1 %all-to-all-start = ((bf16[8,128,2048]{2,1,0:T(8,128)(2,1)}), bf16[8,128,2048]{2,1,0:T(8,128)(2,1)}, u32[]{:S(2)}, u32[]{:S(2)}) async-start(bf16[8,128,2048]{2,1,0:T(8,128)(2,1)} %bitcast.7), calls=%async_computation | async-start | bytes 8388608 | tf_op jit(solution)/shard_map/all_to_all | solution.py:63
  127.3 216.9 %copy-start.8 = (f32[4,704]{1,0:T(4,128)}, f32[4,704]{1,0:T(4,128)S(1)}, u32[]{:S(2)}) copy-start(f32[4,704]{1,0:T(4,128)S(1)} %broadcast_multiply_fusion) | copy-start | bytes 33796
Sparse Core Ops, SparseCore 0:
  11.1 97.5 all-gather.1
  112.7 224.7 reduce-scatter.3
